TPU v7x, 32 devices: a whole 2x2x4 slice. The times are simulated.
32 devices in a mesh: sp: 8 (over z, y), tp: 4 (over x, core).
Axes of the slice: x: 2, y: 2, z: 4, core: 2. Of those that a mesh axis runs over, the one named last changes fastest.
Arguments:
- residual: bfloat16 [4096, 2048], P(('sp', 'tp')), may hold values from -6 to 6
- query_major: bfloat16 [4096, 1024], P('sp', 'tp'), may hold values from -160 to 160
- keys_major: bfloat16 [4096, 1024], P('sp', 'tp'), may hold values from -6.5 to 6.5
- values_major: bfloat16 [4096, 1024], P('sp', 'tp'), may hold values from -6 to 6
- query_minor: bfloat16 [4096, 512], P('sp', 'tp'), may hold values from -160 to 160
- keys_minor: bfloat16 [4096, 512], P('sp', 'tp'), may hold values from -6.5 to 6.5
- values_minor: bfloat16 [4096, 512], P('sp', 'tp'), may hold values from -6 to 6
- lambda_major: float32 [8], P('tp'), may hold values from 0.3 to 0.8
- lambda_minor: float32 [8], P('tp'), may hold values from 0.3 to 0.8
- gain_major: float32 [128], replicated, may hold values from 0.1 to 1.9
- gain_minor: float32 [64], replicated, may hold values from 0.1 to 1.9
- output_major: bfloat16 [1024, 2048], P('tp'), may hold values from -0.15625 to 0.15625
- output_minor: bfloat16 [512, 2048], P('tp'), may hold values from -0.15625 to 0.15625
- mixer_gain: float32 [2048], replicated, may hold values from 0.1 to 1.9
- up_weight: bfloat16 [2048, 8192], P('sp', 'tp'), may hold values from -0.125 to 0.125
- down_weight: bfloat16 [8192, 2048], P('tp', 'sp'), may hold values from -0.0625 to 0.0625
Outputs:
- layer_out: bfloat16 [4096, 2048], P(('sp', 'tp'))
All inputs are finite; a program needn't handle non-finite values.
Results may differ from a plain program's by a relative error of at most 0.018.
Values may be sent and summed in bfloat16 or wider, within the bound.
A program may use at most 128 MiB of HBM per device.

v0:
```python
import jax
import jax.numpy as jnp
from jax import lax
from jax.sharding import PartitionSpec as P

DK_MAJOR = 64
DK_MINOR = 32
SEGMENT = 64


EPSILON = 1e-06
NEGATIVE = -1e30


def swapped(value, axis, stride):
    mask = 2**stride
    pairs = [(source, source ^ mask) for source in range(lax.axis_size(axis))]
    return lax.ppermute(value, axis, pairs)


def to_wire(value):
    return lax.optimization_barrier(value.astype(jnp.bfloat16)).astype(jnp.float32)


def fresh(head_count, query_count, value_size):
    return (
        jnp.full((head_count, 2, query_count), NEGATIVE, jnp.float32),
        jnp.zeros((head_count, 2, query_count), jnp.float32),
        jnp.zeros((head_count, 2, query_count, value_size), jnp.float32),
    )


def fold_piece(carried, queries, key_rows, values, query_pos, key_size):
    head_count = key_rows.shape[1] // (2 * key_size)
    value_size = values.shape[1] // head_count
    query_count = queries.shape[0]
    block_len = min(key_rows.shape[0], query_count)
    query_heads = queries.reshape(query_count, head_count, 2, key_size)
    last_segment = query_pos[query_count - 1] // SEGMENT

    def visit(block_id, carried_in):
        key_first = block_id * block_len

        def update(running):
            peak_old, total_old, accum_old = running
            keys_block = lax.dynamic_slice_in_dim(key_rows, key_first, block_len, 0)
            keys_block = keys_block.reshape(block_len, head_count, 2, key_size)
            values_block = lax.dynamic_slice_in_dim(values, key_first, block_len, 0)
            values_block = values_block.reshape(block_len, head_count, value_size)
            key_pos = key_first + jnp.arange(block_len, dtype=jnp.int32)
            visible = key_pos[None, :] // SEGMENT <= query_pos[:, None] // SEGMENT
            scores = jnp.einsum(
                "qhmd,khmd->hmqk", query_heads, keys_block, preferred_element_type=jnp.float32
            ) * key_size ** (-0.5)
            scores = jnp.where(visible, scores, NEGATIVE)
            peak_new = jnp.maximum(peak_old, jnp.max(scores, axis=-1))
            weights = jnp.where(visible, jnp.exp(scores - peak_new[..., None]), 0.0)
            factor = jnp.exp(peak_old - peak_new)
            total_new = total_old * factor + jnp.sum(weights, axis=-1)
            accum_new = accum_old * factor[..., None] + jnp.einsum(
                "hmqk,khe->hmqe",
                weights.astype(jnp.bfloat16),
                values_block,
                preferred_element_type=jnp.float32,
            )
            return (peak_new, total_new, accum_new)

        def unchanged(running):
            return running

        block_segment = key_first // SEGMENT
        return lax.cond(block_segment <= last_segment, update, unchanged, carried_in)

    return lax.fori_loop(0, key_rows.shape[0] // block_len, visit, carried)


def finish(carried, lambdas, scaling):
    peak_unused, totals, accum = carried
    output = (
        accum[:, 0] / totals[:, 0, :, None]
        - lambdas[:, None, None] * accum[:, 1] / totals[:, 1, :, None]
    )
    output = (
        output * lax.rsqrt(jnp.mean(output * output, axis=-1, keepdims=True) + EPSILON) * scaling
    )
    head_count, query_count, value_size = output.shape
    return (
        jnp.transpose(output, (1, 0, 2))
        .reshape(query_count, head_count * value_size)
        .astype(jnp.bfloat16)
    )


def normalize(stream, scaling):
    normed = (
        stream * lax.rsqrt(jnp.mean(stream * stream, axis=-1, keepdims=True) + EPSILON) * scaling
    )
    return normed.astype(jnp.bfloat16)


def body(
    residual,
    query_major,
    keys_major,
    values_major,
    query_minor,
    keys_minor,
    values_minor,
    lambda_major,
    lambda_minor,
    gain_major,
    gain_minor,
    output_major,
    output_minor,
    mixer_gain,
    up_weight,
    down_weight,
):
    query_count = query_major.shape[0]
    half_rows = query_count // 2
    own_index = lax.axis_index("sp")
    sp_count = lax.axis_size("sp")
    sp_bits = sp_count.bit_length() - 1
    width_major = query_major.shape[1]
    early_pos = own_index * query_count + jnp.arange(half_rows, dtype=jnp.int32)
    early_major = query_major[:half_rows]
    early_minor = query_minor[:half_rows]
    late_queries = jnp.concatenate([query_major[half_rows:], query_minor[half_rows:]], axis=1)
    for bit_number in range(sp_bits):
        late_queries = swapped(late_queries, "sp", bit_number)
    late_major = late_queries[:, :width_major]
    late_minor = late_queries[:, width_major:]
    late_pos = (
        (sp_count - 1 - own_index) * query_count
        + half_rows
        + jnp.arange(half_rows, dtype=jnp.int32)
    )
    heads_major = keys_major.shape[1] // (2 * DK_MAJOR)
    heads_minor = keys_minor.shape[1] // (2 * DK_MINOR)
    size_major = values_major.shape[1] // heads_major
    size_minor = values_minor.shape[1] // heads_minor
    init_major = (
        fresh(heads_major, half_rows, size_major),
        fresh(heads_major, half_rows, size_major),
    )
    init_minor = (
        fresh(heads_minor, half_rows, size_minor),
        fresh(heads_minor, half_rows, size_minor),
    )
    pieces = (
        lax.all_gather(keys_major, "sp", axis=0, tiled=True),
        lax.all_gather(values_major, "sp", axis=0, tiled=True),
    )
    fold_pieces = (
        lax.all_gather(keys_minor, "sp", axis=0, tiled=True),
        lax.all_gather(values_minor, "sp", axis=0, tiled=True),
    )
    first_major = finish(
        fold_piece(init_major[0], early_major, pieces[0], pieces[1], early_pos, DK_MAJOR),
        lambda_major,
        gain_major,
    )
    first_minor = finish(
        fold_piece(init_minor[0], early_minor, fold_pieces[0], fold_pieces[1], early_pos, DK_MINOR),
        lambda_minor,
        gain_minor,
    )
    second_major = finish(
        fold_piece(init_major[1], late_major, pieces[0], pieces[1], late_pos, DK_MAJOR),
        lambda_major,
        gain_major,
    )
    second_minor = finish(
        fold_piece(init_minor[1], late_minor, fold_pieces[0], fold_pieces[1], late_pos, DK_MINOR),
        lambda_minor,
        gain_minor,
    )
    out_width = second_major.shape[1]
    late_out = jnp.concatenate([second_major, second_minor], axis=1)
    for bit_number in range(sp_bits):
        late_out = swapped(late_out, "sp", bit_number)
    second_major = late_out[:, :out_width]
    second_minor = late_out[:, out_width:]
    out_major = jnp.concatenate([first_major, second_major], axis=0)
    out_minor = jnp.concatenate([first_minor, second_minor], axis=0)
    partial_sum = jnp.dot(out_major, output_major, preferred_element_type=jnp.float32)
    partial_sum = partial_sum + jnp.dot(out_minor, output_minor, preferred_element_type=jnp.float32)
    mixed = lax.psum_scatter(
        to_wire(partial_sum).astype(jnp.bfloat16), "tp", scatter_dimension=0, tiled=True
    ).astype(jnp.float32)
    stream = residual.astype(jnp.float32) + mixed
    normed_all = lax.all_gather(normalize(stream, mixer_gain), "tp", axis=0, tiled=True)
    pre_act = jnp.dot(
        normed_all,
        lax.all_gather(up_weight, "sp", axis=0, tiled=True),
        preferred_element_type=jnp.float32,
    )
    hidden = jnp.square(jax.nn.relu(pre_act)).astype(jnp.bfloat16)
    down_full = lax.all_gather(down_weight, "sp", axis=1, tiled=True)
    down_sum = lax.psum_scatter(
        to_wire(jnp.dot(hidden, down_full, preferred_element_type=jnp.float32)).astype(
            jnp.bfloat16
        ),
        "tp",
        scatter_dimension=0,
        tiled=True,
    ).astype(jnp.float32)
    return (stream + down_sum).astype(jnp.bfloat16)


def solution(mesh):
    return jax.shard_map(
        body,
        mesh=mesh,
        in_specs=(
            P(("sp", "tp"), None),
            P("sp", "tp"),
            P("sp", "tp"),
            P("sp", "tp"),
            P("sp", "tp"),
            P("sp", "tp"),
            P("sp", "tp"),
            P("tp"),
            P("tp"),
            P(),
            P(),
            P("tp", None),
            P("tp", None),
            P(),
            P("sp", "tp"),
            P("tp", "sp"),
        ),
        out_specs=P(("sp", "tp"), None),
        check_vma=False,
    )
```

profile of v0, /device:TPU:16, one launch (start us, length us, event | category | flops | bytes accessed | tf_op | source)
XLA Modules:
  0.0 629.8 jit_solution(7971657574266542645)
XLA Ops:
  17.3 6.5 %collective-permute-done = bf16[256,384]{1,0:T(8,128)(2,1)S(1)} collective-permute-done((bf16[256,384]{1,0:T(8,128)(2,1)S(1)}, bf16[256,384]{1,0:T(8,128)(2,1)S(1)}, u32[]{:S(2)}, u32[]{:S(2)}) %collective-permute-start) | collective-permute-done | bytes 196640 | tf_op jit(solution)/shard_map/ppermute | solution.py:18
  25.4 5.5 collective-permute-done.1
  37.6 2.5 collective-permute-done.2
  40.3 11.3 %all-gather.12.cloned.1.call-done = bf16[4096,128]{0,1:T(8,128)(2,1)} async-done(((bf16[512,128]{0,1:T(8,128)(2,1)}), bf16[4096,128]{0,1:T(8,128)(2,1)}) %all-gather.12.cloned.1.call-update) | async-done | bytes 1048592 | tf_op jit(solution)/shard_map/all_gather | solution.py:155
  51.7 43.0 %all-gather.14.cloned.1.call-done = bf16[4096,128]{0,1:T(8,128)(2,1)} async-done(((bf16[512,128]{0,1:T(8,128)(2,1)}), bf16[4096,128]{0,1:T(8,128)(2,1)}) %all-gather.14.cloned.1.call-update) | async-done | bytes 1048592 | tf_op jit(solution)/shard_map/all_gather | solution.py:156
  94.7 17.4 %while.82 = (s32[]{:T(128)}, f32[2,2,256]{2,1,0:T(2,128)S(1)}, f32[2,2,256]{2,1,0:T(2,128)S(1)}, f32[2,2,256,64]{2,3,1,0:T(8,128)S(1)}, s32[]{:T(128)}, /*index=...) while((s32[]{:T(128)}, f32[2,2,256]{2,1,0:T(2,128)S(1)}, ...), condition=%wide.region_19.20_spmd.clone, body=%wide.region_14.19_spmd.clone.sunk | while | flops 52897816 | bytes 4463083 | solution.py:74
  94.7 2.0 conditional.14
  98.9 2.0 conditional.14
  105.2 2.0 conditional.14
  109.4 2.0 conditional.14
  112.1 19.4 %while.83 = (s32[]{:T(128)}, f32[2,2,256]{2,1,0:T(2,128)S(1)}, f32[2,2,256]{2,1,0:T(2,128)S(1)}, f32[2,2,256,64]{2,3,1,0:T(8,128)S(1)}, s32[]{:T(128)}, /*index=...) while((s32[]{:T(128)}, f32[2,2,256]{2,1,0:T(2,128)S(1)}, ...), condition=%wide.region_26.27_spmd.clone, body=%wide.region_21.26_spmd.clone.sunk | while | flops 52897816 | bytes 4463083 | solution.py:74
  112.2 2.0 conditional.15
  116.4 2.0 conditional.15
  124.7 2.0 conditional.15
  128.9 2.0 conditional.15
  131.8 14.5 %all-gather.10.cloned.1.call-done = bf16[4096,256]{0,1:T(8,128)(2,1)} async-done(((bf16[512,256]{0,1:T(8,128)(2,1)}), bf16[4096,256]{0,1:T(8,128)(2,1)}) %all-gather.10.cloned.1.call-update) | async-done | bytes 2097168 | tf_op jit(solution)/shard_map/all_gather | solution.py:152
  146.3 50.5 %all-gather.8.cloned.1.call-done = bf16[4096,256]{0,1:T(8,128)(2,1)} async-done(((bf16[512,256]{0,1:T(8,128)(2,1)}), bf16[4096,256]{0,1:T(8,128)(2,1)}) %all-gather.8.cloned.1.call-update) | async-done | bytes 2097168 | tf_op jit(solution)/shard_map/all_gather | solution.py:151
  196.8 19.9 %while.81 = (s32[]{:T(128)}, f32[2,2,256]{2,1,0:T(2,128)S(1)}, f32[2,2,256]{2,1,0:T(2,128)S(1)}, f32[2,2,256,128]{3,2,1,0:T(8,128)S(1)}, s32[]{:T(128)}, /*index...) while((s32[]{:T(128)}, f32[2,2,256]{2,1,0:T(2,128)S(1)}, ...), condition=%wide.region_12.13_spmd.clone, body=%wide.region_7.12_spmd.clone.sunk | while | flops 103360528 | bytes 5446123 | solution.py:74
  196.9 2.3 conditional.13
  199.3 2.3 conditional.13
  201.7 2.3 conditional.13
  204.1 2.3 conditional.13
  206.5 2.3 conditional.13
  208.9 2.3 conditional.13
  211.3 2.3 conditional.13
  213.7 2.3 conditional.13
  216.8 22.2 %while.80 = (s32[]{:T(128)}, f32[2,2,256]{2,1,0:T(2,128)S(1)}, f32[2,2,256]{2,1,0:T(2,128)S(1)}, f32[2,2,256,128]{3,2,1,0:T(8,128)S(1)}, s32[]{:T(128)}, /*index...) while((s32[]{:T(128)}, f32[2,2,256]{2,1,0:T(2,128)S(1)}, ...), condition=%wide.region_5.6_spmd.clone, body=%wide.region_0.5_spmd.clone.sunk | while | flops 103360528 | bytes 5446123 | solution.py:74
  216.9 2.3 conditional.12
  219.3 2.3 conditional.12
  221.7 2.3 conditional.12
  224.1 2.3 conditional.12
  226.5 2.3 conditional.12
  228.9 2.3 conditional.12
  231.3 2.3 conditional.12
  233.7 2.3 conditional.12
  236.1 2.3 conditional.12
  241.8 5.4 collective-permute-done.3
  248.4 4.4 collective-permute-done.4
  254.8 6.2 collective-permute-done.5
  261.7 2.1 add_convert_fusion
  263.9 33.3 %reduce-scatter.3.cloned.1.call-done = bf16[128,2048]{1,0:T(8,128)(2,1)} async-done(((bf16[512,2048]{1,0:T(8,128)(2,1)}), bf16[128,2048]{1,0:T(8,128)(2,1)}) %reduce-scatter.3.cloned.1.call-update) | async-done | bytes 524304 | tf_op jit(solution)/shard_map/reduce_scatter | solution.py:188
  298.6 2.0 multiply_convert_fusion.1
  302.4 21.0 %all-gather.16.cloned.1.call-done = bf16[512,2048]{1,0:T(8,128)(2,1)} async-done(((bf16[128,2048]{1,0:T(8,128)(2,1)}), bf16[512,2048]{1,0:T(8,128)(2,1)}) %all-gather.16.cloned.1.call-update) | async-done | bytes 2097168 | tf_op jit(solution)/shard_map/all_gather | solution.py:192
  323.4 125.7 %all-gather.18.cloned.1.call-done = bf16[2048,2048]{1,0:T(8,128)(2,1)} async-done(((bf16[256,2048]{1,0:T(8,128)(2,1)}), bf16[2048,2048]{1,0:T(8,128)(2,1)}) %all-gather.18.cloned.1.call-update) | async-done | bytes 8388624 | tf_op jit(solution)/shard_map/all_gather | solution.py:195
  449.1 125.2 %all-gather.20.cloned.1.call-done = bf16[2048,2048]{1,0:T(8,128)(2,1)} async-done(((bf16[2048,256]{1,0:T(8,128)(2,1)}), bf16[2048,2048]{1,0:T(8,128)(2,1)}) %all-gather.20.cloned.1.call-update) | async-done | bytes 8388624 | tf_op jit(solution)/shard_map/all_gather | solution.py:199
  574.3 16.5 %convolution_convert_fusion = bf16[512,2048]{1,0:T(8,128)(2,1)} fusion(bf16[2048,2048]{1,0:T(8,128)(2,1)} %all-gather.20.cloned.1.call-done, bf16[512,2048]{1,0:T(8,128)(2,1)} %all-gather.16.cloned.1.call-done, bf16[2048,2048]{1,0:T(8,128)(2,1)} %all-gather.18.cloned.1.call-done), kind=kOutput, calls=%fused_computation.102 | convolution fusion | flops 8594128896 | bytes 20971520 | tf_op jit(solution)/shard_map/dot_general | solution.py:201
  590.8 30.4 %reduce-scatter.5.cloned.1.call-done = bf16[128,2048]{1,0:T(8,128)(2,1)} async-done(((bf16[512,2048]{1,0:T(8,128)(2,1)}), bf16[128,2048]{1,0:T(8,128)(2,1)}) %reduce-scatter.5.cloned.1.call-update) | async-done | bytes 524304 | tf_op jit(solution)/shard_map/reduce_scatter | solution.py:200
  621.2 2.1 add_convert_fusion.1
  (500 shorter events, 115.0 us)
Async XLA Ops:
  6.5 255.2 %copy-start = (bf16[256,2048]{1,0:T(8,128)(2,1)S(1)}, bf16[256,2048]{1,0:T(8,128)(2,1)}, u32[]{:S(2)}) copy-start(bf16[256,2048]{1,0:T(8,128)(2,1)} %param.43) | copy-start | bytes 3145732
  6.5 45.1 %all-gather.12.cloned.1.call-start = ((), (), s32[]{:S(2)}) async-start(), calls=%async_computation.4 | async-start | bytes 1179648 | tf_op jit(solution)/shard_map/all_gather | solution.py:155
  8.3 86.3 %all-gather.14.cloned.1.call-start = ((), (), s32[]{:S(2)}) async-start(), calls=%async_computation.5 | async-start | bytes 1179648 | tf_op jit(solution)/shard_map/all_gather | solution.py:156
  10.1 136.2 %all-gather.10.cloned.1.call-start = ((), (), s32[]{:S(2)}) async-start(), calls=%async_computation.3 | async-start | bytes 2359296 | tf_op jit(solution)/shard_map/all_gather | solution.py:152
  11.9 184.8 %all-gather.8.cloned.1.call-start = ((), (), s32[]{:S(2)}) async-start(), calls=%async_computation.2 | async-start | bytes 2359296 | tf_op jit(solution)/shard_map/all_gather | solution.py:151
  13.8 283.4 %reduce-scatter.3.cloned.1.call-start = ((), (), s32[]{:S(2)}) async-start(), calls=%async_computation.6 | async-start | bytes 2621440 | tf_op jit(solution)/shard_map/reduce_scatter | solution.py:188
  15.8 8.1 %collective-permute-start = (bf16[256,384]{1,0:T(8,128)(2,1)S(1)}, bf16[256,384]{1,0:T(8,128)(2,1)S(1)}, u32[]{:S(2)}, u32[]{:S(2)}) collective-permute-start(bf16[256,384]{1,0:T(8,128)(2,1)S(1)} %pad_maximum_fusion), channel_id=1, source_target_pairs={{0,4},{4,0},{8,12},{12,8},{16,20},{20,16},{24,28},{28,24},{1,5},{5... | collective-permute-start | bytes 589832 | tf_op jit(solution)/shard_map/ppermute | solution.py:18
  23.9 7.1 %collective-permute-start.1 = (bf16[256,384]{1,0:T(8,128)(2,1)S(1)}, bf16[256,384]{1,0:T(8,128)(2,1)S(1)}, u32[]{:S(2)}, u32[]{:S(2)}) collective-permute-start(bf16[256,384]{1,0:T(8,128)(2,1)S(1)} %collective-permute-done), channel_id=1, source_target_pairs={{0,8},{4,12},{8,0},{12,4},{16,24},{20,28},{24,16},{28,20},{1,9},{5... | collective-permute-start | bytes 589832 | tf_op jit(solution)/shard_map/ppermute | solution.py:18
  30.9 9.2 %collective-permute-start.2 = (bf16[256,384]{1,0:T(8,128)(2,1)S(1)}, bf16[256,384]{1,0:T(8,128)(2,1)S(1)}, u32[]{:S(2)}, u32[]{:S(2)}) collective-permute-start(bf16[256,384]{1,0:T(8,128)(2,1)S(1)} %collective-permute-done.1), channel_id=1, source_target_pairs={{0,16},{4,20},{8,24},{12,28},{16,0},{20,4},{24,8},{28,12},{1,17},{... | collective-permute-start | bytes 589832 | tf_op jit(solution)/shard_map/ppermute | solution.py:18
  112.1 19.5 %copy-start.6 = (f32[2]{0:T(128)S(1)}, f32[2]{0:T(128)}, u32[]{:S(2)}) copy-start(f32[2]{0:T(128)} %param.40) | copy-start | bytes 28
  112.1 19.6 %copy-start.5 = (f32[64]{0:T(128)S(1)}, f32[64]{0:T(128)}, u32[]{:S(2)}) copy-start(f32[64]{0:T(128)} %param.42) | copy-start | bytes 772
  239.0 21.9 %copy-start.3 = (bf16[128,2048]{1,0:T(8,128)(2,1)S(1)}, bf16[128,2048]{1,0:T(8,128)(2,1)}, u32[]{:S(2)}) copy-start(bf16[128,2048]{1,0:T(8,128)(2,1)} %param.44) | copy-start | bytes 1572868
  241.1 6.0 collective-permute-start.3
  247.1 5.7 collective-permute-start.4
  252.8 8.1 %collective-permute-start.5 = (bf16[256,384]{0,1:T(8,128)(2,1)S(1)}, bf16[256,384]{0,1:T(8,128)(2,1)S(1)}, u32[]{:S(2)}, u32[]{:S(2)}) collective-permute-start(bf16[256,384]{0,1:T(8,128)(2,1)S(1)} %collective-permute-done.4), channel_id=1, source_target_pairs={{0,16},{4,20},{8,24},{12,28},{16,0},{20,4},{24,8},{28,12},{1,17},{... | collective-permute-start | bytes 589832 | tf_op jit(solution)/shard_map/ppermute | solution.py:18
  261.7 35.5 %copy-start.1 = (bf16[128,2048]{1,0:T(8,128)(2,1)S(1)}, bf16[128,2048]{1,0:T(8,128)(2,1)}, u32[]{:S(2)}) copy-start(bf16[128,2048]{1,0:T(8,128)(2,1)} %param.32) | copy-start | bytes 1572868
  261.7 36.8 %copy-start.4 = (f32[2048]{0:T(1024)S(1)}, f32[2048]{0:T(1024)}, u32[]{:S(2)}) copy-start(f32[2048]{0:T(1024)} %param.45) | copy-start | bytes 24580
  263.9 59.5 %all-gather.16.cloned.1.call-start = ((), (), s32[]{:S(2)}) async-start(), calls=%async_computation.7 | async-start | bytes 2621440 | tf_op jit(solution)/shard_map/all_gather | solution.py:192
  300.6 148.5 %all-gather.18.cloned.1.call-start = ((), (), s32[]{:S(2)}) async-start(), calls=%async_computation.8 | async-start | bytes 9437184 | tf_op jit(solution)/shard_map/all_gather | solution.py:195
  301.4 272.9 %all-gather.20.cloned.1.call-start = ((), (), s32[]{:S(2)}) async-start(), calls=%async_computation.9 | async-start | bytes 9437184 | tf_op jit(solution)/shard_map/all_gather | solution.py:199
  302.1 319.1 %copy-start.2 = (bf16[128,2048]{1,0:T(8,128)(2,1)S(1)}, bf16[128,2048]{1,0:T(8,128)(2,1)}, u32[]{:S(2)}) copy-start(bf16[128,2048]{1,0:T(8,128)(2,1)} %reduce-scatter.3.cloned.1.call-done) | copy-start | bytes 1572868
  302.1 319.1 %reduce-scatter.5.cloned.1.call-start = ((), (), s32[]{:S(2)}) async-start(), calls=%async_computation.10 | async-start | bytes 2621440 | tf_op jit(solution)/shard_map/reduce_scatter | solution.py:200
Sparse Core Ops, SparseCore 0:
  9.4 42.2 all-gather.11
  53.7 40.8 all-gather.13
  96.7 49.5 all-gather.9
  148.2 48.5 all-gather.7
  264.0 33.2 reduce-scatter.2
  300.7 22.5 all-gather.15
  325.5 123.5 all-gather.17
  451.1 123.1 all-gather.19
  591.0 30.2 reduce-scatter.4
where the time goes:
time: 633 us; the launch traced here: 630 us
  waiting for transfers between devices  487 us (77%)
  matrix products  47.3 us (7%)
  local copies, waits for them, and re-layouts  43.5 us (7%)
  other arithmetic  19.2 us (3%)
  between operations  18.8 us (3%)
  starting transfers between devices  7.53 us (1%)
  loops' own time  6.8 us (1%)
    all_gather x1, waiting for transfers between devices, body(): lax.all_gather(up_weight, 'sp', axis=0, tiled=True)  126 us
    all_gather x1, waiting for transfers between devices, body(): down_full = lax.all_gather(down_weight, 'sp', axis=1, tiled=True)  125 us
    all_gather x1, waiting for transfers between devices, body(): lax.all_gather(keys_major, 'sp', axis=0, tiled=True)  50.5 us
    all_gather x1, waiting for transfers between devices, body(): lax.all_gather(values_minor, 'sp', axis=0, tiled=True)  43 us
    reduce_scatter x1, waiting for transfers between devices, body(): lax.psum_scatter(to_wire(partial_sum).astype(jnp.bfloat16), 'tp', scatter...  33.3 us
    dynamic_slice x34, local copies, waits for them, and re-layouts, update(): values_block = lax.dynamic_slice_in_dim(values, key_first, block_len, 0)  32 us
    ppermute x6, waiting for transfers between devices, swapped(): return lax.ppermute(value, axis, pairs)  30.4 us
    reduce_scatter x1, waiting for transfers between devices, body(): lax.psum_scatter(to_wire(jnp.dot(hidden, down_full, preferred_element_typ...  30.4 us
  transfers between devices with their start and end apart: 15, of which 15 were waited for; matrix products, arithmetic and copies ran while one was open for 7% of the time, Pallas kernels for 0%

commit v1 on v0

v1 whole, which is shorter than its diff:
```python
import functools

import jax
import jax.numpy as jnp
from jax import lax
from jax.experimental import pallas as pl
from jax.experimental.pallas import tpu as pltpu
from jax.sharding import PartitionSpec as P

DK_MAJOR = 64
DK_MINOR = 32
SEGMENT = 64
MAPS = 2

EPSILON = 1e-06
NEGATIVE = -1e30
LOG2_E = 1.4426950408889634
ANY = pl.BlockSpec(memory_space=pl.ANY)
VMEM = pl.BlockSpec(memory_space=pltpu.VMEM)
SMEM = pl.BlockSpec(memory_space=pltpu.SMEM)


def to_wire(value):
    return lax.optimization_barrier(value.astype(jnp.bfloat16)).astype(jnp.float32)


def grid_sizes(sp_count):
    y_count = 1 << ((sp_count.bit_length() - 1) // 2)
    return sp_count // y_count, y_count


class Gather:
    def __init__(self, sp_count, places, send_sem, recv_sem):
        self.z_count, self.y_count = grid_sizes(sp_count)
        own = lax.axis_index("sp")
        self.own, self.z, self.y = own, own // self.y_count, lax.rem(own, self.y_count)
        self.places, self.send_sem, self.recv_sem = places, send_sem, recv_sem
        self.copies = []

    def z_peer(self, step):
        return lax.rem(self.z + step, self.z_count) * self.y_count + self.y

    def y_peer(self, step):
        return self.z * self.y_count + lax.rem(self.y + step, self.y_count)

    def send(self, array, source, src_ref, target):
        copy = pltpu.make_async_remote_copy(
            src_ref=src_ref,
            dst_ref=self.places[array](source),
            send_sem=self.send_sem.at[array, len([c for c in self.copies if c[0] == array])],
            recv_sem=self.recv_sem.at[array, source],
            device_id={"sp": target},
            device_id_type=pl.DeviceIdType.MESH,
        )
        copy.start()
        self.copies.append((array, copy))

    def wait_block(self, array, source):
        place = self.places[array](source)
        pltpu.make_async_remote_copy(
            src_ref=place,
            dst_ref=place,
            send_sem=self.send_sem.at[array, 0],
            recv_sem=self.recv_sem.at[array, source],
            device_id={"sp": self.y_peer(1)},
            device_id_type=pl.DeviceIdType.MESH,
        ).wait_recv()

    def send_z(self, array, src_ref):
        for step in range(1, self.z_count):
            self.send(array, self.own, src_ref, self.z_peer(step))

    def send_y(self, array, src_ref):
        for step in range(1, self.y_count):
            self.send(array, self.own, src_ref, self.y_peer(step))

    def pass_on(self, array, step):
        source = self.z_peer(self.z_count - step)
        self.wait_block(array, source)
        for y_step in range(1, self.y_count):
            self.send(array, source, self.places[array](source), self.y_peer(y_step))

    def wait_y(self, array):
        for y_step in range(1, self.y_count):
            for z_step in range(self.z_count):
                z_at = lax.rem(self.z + z_step, self.z_count)
                self.wait_block(array, z_at * self.y_count + lax.rem(self.y + y_step, self.y_count))

    def finish(self):
        for _, copy in self.copies:
            copy.wait_send()


def mixer_kernel(
    sp_count,
    groups,
    q_major,
    k_major,
    v_major,
    q_minor,
    kv_minor,
    lam_major,
    lam_minor,
    gain_major,
    gain_minor,
    up_ref,
    down_ref,
    out_major,
    out_minor,
    up_all,
    down_all,
    k_major_all,
    v_major_all,
    kv_minor_all,
    qm_major,
    qm_minor,
    acc_major,
    acc_minor,
    peaks,
    totals,
    send_sem,
    recv_sem,
    local_sem,
):
    rows = q_major.shape[0]
    up_rows = up_ref.shape[0]

    def rows_of(ref, count):
        return lambda source: ref.at[pl.ds(pl.multiple_of(source * count, count), count), :]

    places = [
        rows_of(k_major_all, rows),
        rows_of(v_major_all, rows),
        rows_of(kv_minor_all, rows),
        rows_of(up_all, up_rows),
        lambda source: down_all.at[source],
    ]
    own_refs = [k_major, v_major, kv_minor, up_ref, down_ref]
    gather = Gather(sp_count, places, send_sem, recv_sem)
    own = gather.own

    barrier = pltpu.get_barrier_semaphore()
    peers = [gather.z_peer(step) for step in range(1, gather.z_count)]
    peers += [gather.y_peer(step) for step in range(1, gather.y_count)]
    for peer in peers:
        pl.semaphore_signal(
            barrier, inc=1, device_id={"sp": peer}, device_id_type=pl.DeviceIdType.MESH
        )
    pl.semaphore_wait(barrier, len(peers))

    for array in range(3):
        gather.send_z(array, own_refs[array])
    for array in range(3):
        gather.send_y(array, own_refs[array])
    for array in (3, 4):
        gather.send_z(array, own_refs[array])
    local = []
    for slot, array in enumerate((3, 4)):
        copy = pltpu.make_async_copy(own_refs[array], places[array](own), local_sem.at[slot])
        copy.start()
        local.append(copy)

    heads = []
    for group, (head_count, key_size) in enumerate(groups):
        q_ref, qm_ref = ((q_major, qm_major), (q_minor, qm_minor))[group]
        acc_ref = (acc_major, acc_minor)[group]
        value_size = acc_ref.shape[1]
        lanes = qm_ref.shape[2]
        for head in range(head_count):
            first = head * MAPS * key_size
            lane_first = first // lanes * lanes
            block = q_ref[:, lane_first : lane_first + lanes]
            lane = lax.broadcasted_iota(jnp.int32, block.shape, 1) + lane_first
            for m in range(MAPS):
                low = first + m * key_size
                keep = (lane >= low) & (lane < low + key_size)
                picked = jnp.where(keep, block.astype(jnp.float32), 0.0).astype(block.dtype)
                qm_ref[head, m * rows : (m + 1) * rows, :] = picked
            heads.append((group, head, len(heads), lane_first, lanes, value_size, key_size))

    minor_keys = q_minor.shape[1]
    minor_first = minor_keys // 128 * 128

    def fold(key_refs, value_refs, at, diagonal):
        window = pl.ds(at, rows)
        stored = (value_refs[0][window, :], value_refs[1][window, minor_first:])
        turned = [jnp.transpose(v.astype(jnp.float32)).astype(jnp.bfloat16) for v in stored]
        turned[1] = turned[1][minor_keys - minor_first :, :]
        for group, head, index, lane_first, lanes, value_size, key_size in heads:
            qm_ref = (qm_major, qm_minor)[group]
            acc_ref = (acc_major, acc_minor)[group]
            keys = key_refs[group][window, lane_first : lane_first + lanes]
            values = turned[group][head * value_size : (head + 1) * value_size, :]
            scores = lax.dot_general(
                keys, qm_ref[head], (((1,), (1,)), ((), ())), preferred_element_type=jnp.float32
            ) * (key_size ** (-0.5) * LOG2_E)
            if diagonal:
                key_pos = lax.broadcasted_iota(jnp.int32, scores.shape, 0)
                query_pos = lax.broadcasted_iota(jnp.int32, scores.shape, 1) % rows
                visible = key_pos // SEGMENT <= query_pos // SEGMENT
                scores = jnp.where(visible, scores, NEGATIVE)
            peak = jnp.max(scores, axis=0, keepdims=True)
            if not diagonal:
                peak_old = peaks[index]
                peak = jnp.maximum(peak, peak_old)
            weights = jnp.exp2(scores - peak)
            total = jnp.sum(weights, axis=0, keepdims=True)
            sums = jnp.dot(
                values, weights.astype(jnp.bfloat16), preferred_element_type=jnp.float32
            )
            if not diagonal:
                factor = jnp.exp2(peak_old - peak)
                total = total + totals[index] * factor
                sums = sums + acc_ref[head] * factor
            peaks[index] = peak
            totals[index] = total
            acc_ref[head] = sums

    fold((k_major, kv_minor), (v_major, kv_minor), 0, True)

    for step in range(1, gather.z_count):
        for array in range(3):
            gather.pass_on(array, step)
    for array in (3, 4):
        gather.send_y(array, own_refs[array])
    for array in range(3):
        gather.wait_y(array)

    def earlier(block, carry):
        at = pl.multiple_of(block * rows, rows)
        fold((k_major_all, kv_minor_all), (v_major_all, kv_minor_all), at, False)
        return carry

    lax.fori_loop(0, own, earlier, 0)

    for group, (head_count, _) in enumerate(groups):
        acc_ref = (acc_major, acc_minor)[group]
        lam_ref = (lam_major, lam_minor)[group]
        gain_ref = (gain_major, gain_minor)[group]
        out_ref = (out_major, out_minor)[group]
        done = []
        for head in range(head_count):
            index = next(h[2] for h in heads if h[0] == group and h[1] == head)
            ratio = acc_ref[head] / totals[index]
            diff = ratio[:, :rows] - lam_ref[head] * ratio[:, rows:]
            mean = jnp.mean(diff * diff, axis=0, keepdims=True)
            done.append(diff * lax.rsqrt(mean + EPSILON) * gain_ref[...])
        out_ref[...] = jnp.transpose(jnp.concatenate(done, axis=0)).astype(out_ref.dtype)

    for step in range(1, gather.z_count):
        for array in (3, 4):
            gather.pass_on(array, step)
    for array in (3, 4):
        gather.wait_y(array)
    for copy in local:
        copy.wait()
    gather.finish()


def mixer(sp_count, *args):
    q_major, k_major, v_major, q_minor, kv_minor = args[:5]
    up_weight, down_weight = args[9:11]
    heads_major = k_major.shape[1] // (MAPS * DK_MAJOR)
    heads_minor = q_minor.shape[1] // (MAPS * DK_MINOR)
    rows = q_major.shape[0]
    size_major = v_major.shape[1] // heads_major
    width_minor = kv_minor.shape[1] - q_minor.shape[1]
    size_minor = width_minor // heads_minor
    lanes_major = min(MAPS * DK_MAJOR, q_major.shape[1])
    lanes_minor = min(128, q_minor.shape[1])
    z_count, y_count = grid_sizes(sp_count)
    sends = (z_count - 1) + (y_count - 1) * z_count
    tokens = rows * sp_count
    bf16, f32 = jnp.bfloat16, jnp.float32
    head_total = heads_major + heads_minor
    return pl.pallas_call(
        functools.partial(
            mixer_kernel, sp_count, ((heads_major, DK_MAJOR), (heads_minor, DK_MINOR))
        ),
        out_shape=(
            jax.ShapeDtypeStruct(v_major.shape, bf16),
            jax.ShapeDtypeStruct((rows, width_minor), bf16),
            jax.ShapeDtypeStruct((up_weight.shape[0] * sp_count, up_weight.shape[1]), bf16),
            jax.ShapeDtypeStruct((sp_count, *down_weight.shape), bf16),
        ),
        in_specs=[VMEM] * 5 + [SMEM] * 2 + [VMEM] * 4,
        out_specs=(VMEM, VMEM, ANY, ANY),
        scratch_shapes=[
            pltpu.VMEM((tokens, k_major.shape[1]), bf16),
            pltpu.VMEM((tokens, v_major.shape[1]), bf16),
            pltpu.VMEM((tokens, kv_minor.shape[1]), bf16),
            pltpu.VMEM((heads_major, MAPS * rows, lanes_major), bf16),
            pltpu.VMEM((heads_minor, MAPS * rows, lanes_minor), bf16),
            pltpu.VMEM((heads_major, size_major, MAPS * rows), f32),
            pltpu.VMEM((heads_minor, size_minor, MAPS * rows), f32),
            pltpu.VMEM((head_total, 1, MAPS * rows), f32),
            pltpu.VMEM((head_total, 1, MAPS * rows), f32),
            pltpu.SemaphoreType.DMA((5, sends)),
            pltpu.SemaphoreType.DMA((5, sp_count)),
            pltpu.SemaphoreType.DMA((2,)),
        ],
        compiler_params=pltpu.CompilerParams(
            collective_id=0, has_side_effects=True, vmem_limit_bytes=60 * 1024 * 1024
        ),
    )(*args)


def normalize(stream, scaling):
    normed = (
        stream * lax.rsqrt(jnp.mean(stream * stream, axis=-1, keepdims=True) + EPSILON) * scaling
    )
    return normed.astype(jnp.bfloat16)


def body(
    residual,
    query_major,
    keys_major,
    values_major,
    query_minor,
    keys_minor,
    values_minor,
    lambda_major,
    lambda_minor,
    gain_major,
    gain_minor,
    output_major,
    output_minor,
    mixer_gain,
    up_weight,
    down_weight,
):
    out_major, out_minor, up_full, down_full = mixer(
        lax.axis_size("sp"),
        query_major,
        keys_major,
        values_major,
        query_minor,
        jnp.concatenate([keys_minor, values_minor], axis=1),
        lambda_major,
        lambda_minor,
        gain_major[:, None],
        gain_minor[:, None],
        up_weight,
        down_weight,
    )
    partial_sum = jnp.dot(out_major, output_major, preferred_element_type=jnp.float32)
    partial_sum = partial_sum + jnp.dot(out_minor, output_minor, preferred_element_type=jnp.float32)
    mixed = lax.psum_scatter(
        to_wire(partial_sum).astype(jnp.bfloat16), "tp", scatter_dimension=0, tiled=True
    ).astype(jnp.float32)
    stream = residual.astype(jnp.float32) + mixed
    normed_all = lax.all_gather(normalize(stream, mixer_gain), "tp", axis=0, tiled=True)
    pre_act = jnp.dot(
        normed_all,
        up_full,
        preferred_element_type=jnp.float32,
    )
    hidden = jnp.square(jax.nn.relu(pre_act)).astype(jnp.bfloat16)
    down_sum = lax.psum_scatter(
        to_wire(
            jnp.einsum("th,shd->tsd", hidden, down_full, preferred_element_type=jnp.float32)
        )
        .astype(jnp.bfloat16)
        .reshape(stream.shape[0] * lax.axis_size("tp"), -1),
        "tp",
        scatter_dimension=0,
        tiled=True,
    ).astype(jnp.float32)
    return (stream + down_sum).astype(jnp.bfloat16)


def solution(mesh):
    return jax.shard_map(
        body,
        mesh=mesh,
        in_specs=(
            P(("sp", "tp"), None),
            P("sp", "tp"),
            P("sp", "tp"),
            P("sp", "tp"),
            P("sp", "tp"),
            P("sp", "tp"),
            P("sp", "tp"),
            P("tp"),
            P("tp"),
            P(),
            P(),
            P("tp", None),
            P("tp", None),
            P(),
            P("sp", "tp"),
            P("tp", "sp"),
        ),
        out_specs=P(("sp", "tp"), None),
        check_vma=False,
    )
```

time: 633 us -> 479 us (0.76)
  waiting for transfers between devices: 487 us -> 84.2 us
  Pallas kernels: 0 us -> 346 us
  local copies, waits for them, and re-layouts: 43.5 us -> 6.12 us
  matrix products: 47.3 us -> 20.3 us
  other arithmetic: 19.2 us -> 7.12 us
  starting transfers between devices: 7.53 us -> 0.27 us
  loops' own time: 6.8 us -> 0 us
    all_gather x6 -> x0, waiting for transfers between devices: 370 us -> none  [the longest x1 126 us: body(): lax.all_gather(up_weight, 'sp', axis=0, tiled=True)]
    pallas_call x0 -> x1, Pallas kernels: none -> 346 us  [mixer(): pl.pallas_call(functools.partial(mixer_kernel, sp_count, ((heads_major, D...]
    dynamic_slice x34 -> x0, local copies, waits for them, and re-layouts: 32 us -> none  [update(): values_block = lax.dynamic_slice_in_dim(values, key_first, block_len, 0)]
    ppermute x6 -> x0, waiting for transfers between devices: 30.4 us -> none  [swapped(): return lax.ppermute(value, axis, pairs)]
    dot_general x69 -> x1, matrix products: 44.5 us -> 16.5 us  [body(): jnp.einsum('th,shd->tsd', hidden, down_full, preferred_element_type=jnp.f...]
    reduce_sum x36 -> x0, other arithmetic: 8.03 us -> none  [the longest x34 7.07 us: update(): total_new = total_old * factor + jnp.sum(weights, axis=-1)]
    unnamed x22 -> x12, local copies, waits for them, and re-layouts: 7.07 us -> 0.03 us
    ppermute x6 -> x0, starting transfers between devices: 7.02 us -> none  [swapped(): return lax.ppermute(value, axis, pairs)]
  transfers between devices with their start and end apart: 15 -> 3, of which waited for: 15 -> 3; matrix products, arithmetic and copies ran while one was open for 7% -> 0% of each run, Pallas kernels for 0% -> 0%
where the time goes in v1:
time: 479 us; the launch traced here: 477 us
  Pallas kernels  346 us (72%)
  waiting for transfers between devices  84.2 us (18%)
  matrix products  20.3 us (4%)
  between operations  13.2 us (3%)
  other arithmetic  7.12 us (1%)
  local copies, waits for them, and re-layouts  6.12 us (1%)
    pallas_call x1, Pallas kernels, mixer(): pl.pallas_call(functools.partial(mixer_kernel, sp_count, ((heads_major, D...  346 us
    reduce_scatter x1, waiting for transfers between devices, body(): lax.psum_scatter(to_wire(jnp.einsum('th,shd->tsd', hidden, down_full, pre...  31.3 us
    reduce_scatter x1, waiting for transfers between devices, body(): lax.psum_scatter(to_wire(partial_sum).astype(jnp.bfloat16), 'tp', scatter...  30.4 us
    all_gather x1, waiting for transfers between devices, body(): lax.all_gather(normalize(stream, mixer_gain), 'tp', axis=0, tiled=True)  22.5 us
    dot_general x1, matrix products, body(): jnp.einsum('th,shd->tsd', hidden, down_full, preferred_element_type=jnp.f...  16.5 us
  transfers between devices with their start and end apart: 3, of which 3 were waited for; matrix products, arithmetic and copies ran while one was open for 0% of the time, Pallas kernels for 0%

profile of v1, /device:TPU:16, one launch (start us, length us, event | category | flops | bytes accessed | tf_op | source)
XLA Modules:
  0.0 477.2 jit_solution(1589054389989290798)
XLA Ops:
  6.5 0.0 copy-start
  6.5 0.0 reduce-scatter.3.cloned.1.call-start
  6.5 1.4 copy.18.gain_minor
  8.0 1.4 copy.17.gain_major
  9.4 1.7 pad_maximum_fusion.kv_minor
  11.1 345.9 %shard_map.154 = (bf16[512,256]{1,0:T(8,128)(2,1)}, bf16[512,128]{1,0:T(8,128)(2,1)}, bf16[2048,2048]{1,0:T(8,128)(2,1)}, bf16[8,2048,256]{2,1,0:T(8,128)(2,1)}) custom-call(bf16[512,256]{1,0:T(8,128)(2,1)} %q_major.1, bf16[512,256]{1,0:T(8,128)(2,1)} %k_major.1, bf16[512,256]{1,0:T(8,128)(2,1)} %v_major.1, bf16[512,128]{1,0:T(8,128)(2,1)} %q_minor.1, ...), custom_call_target="tpu_custom_call" | custom-call | tf_op jit(solution)/shard_map/pallas_call | solution.py:276
  357.0 0.0 copy-start.3
  357.0 0.0 copy-start.4
  357.0 0.0 copy-done
  357.0 1.7 fusion.2
  358.8 0.0 copy-done.3
  358.8 0.0 copy-done.4
  358.8 0.0 copy-start.1
  358.8 0.0 copy-start.5
  358.8 2.0 add_convert_fusion
  360.8 0.0 reduce-scatter.3.cloned.1.call-update
  360.9 0.0 all-gather.2.cloned.1.call-start
  360.9 30.4 %reduce-scatter.3.cloned.1.call-done = bf16[128,2048]{1,0:T(8,128)(2,1)} async-done(((bf16[512,2048]{1,0:T(8,128)(2,1)}), bf16[128,2048]{1,0:T(8,128)(2,1)}) %reduce-scatter.3.cloned.1.call-update) | async-done | bytes 524304 | tf_op jit(solution)/shard_map/reduce_scatter | solution.py:349
  391.3 0.0 copy-done.1
  391.3 1.3 multiply_reduce_fusion
  392.6 0.0 copy-done.5
  392.6 2.0 multiply_convert_fusion.1
  394.6 0.0 all-gather.2.cloned.1.call-update
  394.7 0.2 reduce-scatter.5.cloned.1.call-start
  394.9 22.5 %all-gather.2.cloned.1.call-done = bf16[512,2048]{1,0:T(8,128)(2,1)} async-done(((bf16[128,2048]{1,0:T(8,128)(2,1)}), bf16[512,2048]{1,0:T(8,128)(2,1)}) %all-gather.2.cloned.1.call-update) | async-done | bytes 2097168 | tf_op jit(solution)/shard_map/all_gather | solution.py:353
  417.4 16.5 %convolution_convert_fusion = bf16[512,8,256]{2,0,1:T(8,128)(2,1)} fusion(bf16[8,2048,256]{2,1,0:T(8,128)(2,1)} %get-tuple-element.12, bf16[512,2048]{1,0:T(8,128)(2,1)} %all-gather.2.cloned.1.call-done, bf16[2048,2048]{1,0:T(8,128)(2,1)} %get-tuple-element.11), kind=kOutput, calls=%fused_computation.3 | convolution fusion | flops 8594128896 | bytes 20971520 | tf_op jit(solution)/shard_map/th,shd->tsd/dot_general | solution.py:362
  433.9 0.0 copy-start.2
  433.9 3.3 copy.20
  437.2 0.0 reduce-scatter.5.cloned.1.call-update
  437.2 31.3 %reduce-scatter.5.cloned.1.call-done = bf16[128,2048]{1,0:T(8,128)(2,1)} async-done(((bf16[512,2048]{1,0:T(8,128)(2,1)}), bf16[128,2048]{1,0:T(8,128)(2,1)}) %reduce-scatter.5.cloned.1.call-update) | async-done | bytes 524304 | tf_op jit(solution)/shard_map/reduce_scatter | solution.py:360
  468.6 0.0 copy-done.2
  468.6 2.1 add_convert_fusion.1
  (1 shorter events, 0.0 us)
Async XLA Ops:
  6.5 350.5 %copy-start = (bf16[256,2048]{1,0:T(8,128)(2,1)S(1)}, bf16[256,2048]{1,0:T(8,128)(2,1)}, u32[]{:S(2)}) copy-start(bf16[256,2048]{1,0:T(8,128)(2,1)} %param.27) | copy-start | bytes 3145732
  6.5 384.7 %reduce-scatter.3.cloned.1.call-start = ((), (), s32[]{:S(2)}) async-start(), calls=%async_computation.2 | async-start | bytes 2621440 | tf_op jit(solution)/shard_map/reduce_scatter | solution.py:349
  357.0 1.8 copy-start.3
  357.0 1.8 copy-start.4
  358.8 32.5 %copy-start.1 = (bf16[128,2048]{1,0:T(8,128)(2,1)S(1)}, bf16[128,2048]{1,0:T(8,128)(2,1)}, u32[]{:S(2)}) copy-start(bf16[128,2048]{1,0:T(8,128)(2,1)} %param.16) | copy-start | bytes 1572868
  358.8 33.8 %copy-start.5 = (f32[2048]{0:T(1024)S(1)}, f32[2048]{0:T(1024)}, u32[]{:S(2)}) copy-start(f32[2048]{0:T(1024)} %param.29) | copy-start | bytes 24580
  360.9 56.5 %all-gather.2.cloned.1.call-start = ((), (), s32[]{:S(2)}) async-start(), calls=%async_computation.3 | async-start | bytes 2621440 | tf_op jit(solution)/shard_map/all_gather | solution.py:353
  394.7 73.9 %reduce-scatter.5.cloned.1.call-start = ((), (), s32[]{:S(2)}) async-start(), calls=%async_computation.4 | async-start | bytes 2621440 | tf_op jit(solution)/shard_map/reduce_scatter | solution.py:360
  433.9 34.6 %copy-start.2 = (bf16[128,2048]{1,0:T(8,128)(2,1)S(1)}, bf16[128,2048]{1,0:T(8,128)(2,1)}, u32[]{:S(2)}) copy-start(bf16[128,2048]{1,0:T(8,128)(2,1)} %reduce-scatter.3.cloned.1.call-done) | copy-start | bytes 1572868
Sparse Core Ops, SparseCore 0:
  361.0 30.2 reduce-scatter.2
  394.8 22.5 all-gather.1
  437.3 31.1 reduce-scatter.4

commit v2 on v1

--- a/solution.py
+++ b/solution.py
@@ -18,10 +18,6 @@
 ANY = pl.BlockSpec(memory_space=pl.ANY)
 VMEM = pl.BlockSpec(memory_space=pltpu.VMEM)
 SMEM = pl.BlockSpec(memory_space=pltpu.SMEM)
-
-
-def to_wire(value):
-    return lax.optimization_barrier(value.astype(jnp.bfloat16)).astype(jnp.float32)
 
 
 def grid_sizes(sp_count):
@@ -154,6 +150,8 @@
         gather.send_y(array, own_refs[array])
     for array in (3, 4):
         gather.send_z(array, own_refs[array])
+    for array in (3, 4):
+        gather.send_y(array, own_refs[array])
     local = []
     for slot, array in enumerate((3, 4)):
         copy = pltpu.make_async_copy(own_refs[array], places[array](own), local_sem.at[slot])
@@ -221,17 +219,26 @@
     for step in range(1, gather.z_count):
         for array in range(3):
             gather.pass_on(array, step)
-    for array in (3, 4):
-        gather.send_y(array, own_refs[array])
-    for array in range(3):
-        gather.wait_y(array)
 
     def earlier(block, carry):
         at = pl.multiple_of(block * rows, rows)
         fold((k_major_all, kv_minor_all), (v_major_all, kv_minor_all), at, False)
         return carry
 
-    lax.fori_loop(0, own, earlier, 0)
+    y_count = gather.y_count
+
+    def same_y(z_at, carry):
+        return earlier(z_at * y_count + gather.y, carry)
+
+    def other_y(index, carry):
+        z_at, place = index // (y_count - 1), lax.rem(index, y_count - 1)
+        y_at = place + (place >= gather.y).astype(jnp.int32)
+        return earlier(z_at * y_count + y_at, carry)
+
+    lax.fori_loop(0, gather.z, same_y, 0)
+    for array in range(3):
+        gather.wait_y(array)
+    lax.fori_loop(0, gather.z * (y_count - 1) + gather.y, other_y, 0)
 
     for group, (head_count, _) in enumerate(groups):
         acc_ref = (acc_major, acc_minor)[group]
@@ -305,11 +312,125 @@
     )(*args)
 
 
-def normalize(stream, scaling):
-    normed = (
-        stream * lax.rsqrt(jnp.mean(stream * stream, axis=-1, keepdims=True) + EPSILON) * scaling
-    )
-    return normed.astype(jnp.bfloat16)
+class Exchange:
+    def __init__(self, tp_count, send_sem, recv_sem):
+        own = lax.axis_index("tp")
+        self.x_count = tp_count // 2
+        self.own, self.x, self.core = own, own // 2, lax.rem(own, 2)
+        self.partner = self.x * 2 + 1 - self.core
+        self.send_sem, self.recv_sem = send_sem, recv_sem
+
+    def enter(self):
+        barrier = pltpu.get_barrier_semaphore()
+        peers = [self.partner] + [self.x_peer(step) for step in range(1, self.x_count)]
+        for peer in peers:
+            pl.semaphore_signal(
+                barrier, inc=1, device_id={"tp": peer}, device_id_type=pl.DeviceIdType.MESH
+            )
+        pl.semaphore_wait(barrier, len(peers))
+
+    def x_peer(self, step):
+        return lax.rem(self.x + step, self.x_count) * 2 + self.core
+
+    def copy(self, src, dst, slot, target):
+        made = pltpu.make_async_remote_copy(
+            src_ref=src,
+            dst_ref=dst,
+            send_sem=self.send_sem.at[slot],
+            recv_sem=self.recv_sem.at[slot],
+            device_id={"tp": target},
+            device_id_type=pl.DeviceIdType.MESH,
+        )
+        made.start()
+        return made
+
+    def total(self, partial, pair_in, pair_sum, x_in, rows):
+        def block(x_at, core):
+            return pl.ds(pl.multiple_of((x_at * 2 + core) * rows, rows), rows)
+
+        steps = list(range(1, self.x_count)) + [0]
+        at = [lax.rem(self.x + step, self.x_count) for step in range(self.x_count)]
+        pair = {}
+        for step in steps:
+            pair[step] = self.copy(
+                partial.at[block(at[step], 1 - self.core), :], pair_in.at[step], step, self.partner
+            )
+        across = []
+        for step in steps:
+            pair[step].wait_recv()
+            mine = partial[block(at[step], self.core), :].astype(jnp.float32)
+            both = mine + pair_in[step].astype(jnp.float32)
+            if step:
+                pair_sum[step] = both.astype(jnp.bfloat16)
+                across.append(
+                    self.copy(
+                        pair_sum.at[step], x_in.at[step], self.x_count + step, self.x_peer(step)
+                    )
+                )
+        for made in across:
+            made.wait_recv()
+        for step in range(1, self.x_count):
+            both = both + x_in[step].astype(jnp.float32)
+        return both, list(pair.values()) + across
+
+
+def mix_kernel(
+    tp_count, partial, residual, gain, stream_ref, normed_ref, pair_in, pair_sum, x_in, held, send_sem, recv_sem
+):
+    exchange = Exchange(tp_count, send_sem, recv_sem)
+    exchange.enter()
+    rows = residual.shape[0]
+    mixed, copies = exchange.total(partial, pair_in, pair_sum, x_in, rows)
+    stream = residual[...].astype(jnp.float32) + mixed
+    stream_ref[...] = stream
+    mean = jnp.mean(stream * stream, axis=-1, keepdims=True)
+    normed = (stream * lax.rsqrt(mean + EPSILON) * gain[...]).astype(jnp.bfloat16)
+    held[...] = normed
+
+    def place(index):
+        return normed_ref.at[pl.ds(pl.multiple_of(index * rows, rows), rows), :]
+
+    base, count = 2 * exchange.x_count, exchange.x_count
+    sent = [exchange.copy(held, place(exchange.own), base + step, exchange.x_peer(step)) for step in range(1, count)]
+    passed = [exchange.copy(held, place(exchange.own), base + count, exchange.partner)]
+    normed_ref[pl.ds(pl.multiple_of(exchange.own * rows, rows), rows), :] = normed
+    for step in range(1, count):
+        sent[step - 1].wait_recv()
+        source = exchange.x_peer(count - step)
+        passed.append(
+            exchange.copy(place(source), place(source), base + count + step, exchange.partner)
+        )
+    for made in passed:
+        made.wait_recv()
+    for made in copies + sent + passed:
+        made.wait_send()
+
+
+def sum_kernel(tp_count, partial, stream, out_ref, pair_in, pair_sum, x_in, send_sem, recv_sem):
+    exchange = Exchange(tp_count, send_sem, recv_sem)
+    exchange.enter()
+    total, copies = exchange.total(partial, pair_in, pair_sum, x_in, stream.shape[0])
+    out_ref[...] = (stream[...] + total).astype(out_ref.dtype)
+    for made in copies:
+        made.wait_send()
+
+
+def tp_call(kernel, identity, inputs, out_shape, rows, holds):
+    tp_count = lax.axis_size("tp")
+    slots = (tp_count // 2, rows, inputs[0].shape[1])
+    held = [pltpu.VMEM(slots[1:], jnp.bfloat16)] if holds else []
+    return pl.pallas_call(
+        functools.partial(kernel, tp_count),
+        out_shape=out_shape,
+        in_specs=[VMEM] * len(inputs),
+        out_specs=jax.tree.map(lambda _: VMEM, out_shape),
+        scratch_shapes=[pltpu.VMEM(slots, jnp.bfloat16)] * 3
+        + held
+        + [pltpu.SemaphoreType.DMA((2 * tp_count,))] * 2,
+        compiler_params=pltpu.CompilerParams(
+            collective_id=identity, has_side_effects=True, vmem_limit_bytes=32 * 1024 * 1024
+        ),
+    )(*inputs)
 
 
 def body(
@@ -346,28 +467,34 @@
     )
     partial_sum = jnp.dot(out_major, output_major, preferred_element_type=jnp.float32)
     partial_sum = partial_sum + jnp.dot(out_minor, output_minor, preferred_element_type=jnp.float32)
-    mixed = lax.psum_scatter(
-        to_wire(partial_sum).astype(jnp.bfloat16), "tp", scatter_dimension=0, tiled=True
-    ).astype(jnp.float32)
-    stream = residual.astype(jnp.float32) + mixed
-    normed_all = lax.all_gather(normalize(stream, mixer_gain), "tp", axis=0, tiled=True)
+    rows = residual.shape[0]
+    stream, normed_all = tp_call(
+        mix_kernel,
+        1,
+        (partial_sum.astype(jnp.bfloat16), residual, mixer_gain[None, :]),
+        (
+            jax.ShapeDtypeStruct(residual.shape, jnp.float32),
+            jax.ShapeDtypeStruct(partial_sum.shape, jnp.bfloat16),
+        ),
+        rows,
+        True,
+    )
     pre_act = jnp.dot(
         normed_all,
         up_full,
         preferred_element_type=jnp.float32,
     )
     hidden = jnp.square(jax.nn.relu(pre_act)).astype(jnp.bfloat16)
-    down_sum = lax.psum_scatter(
-        to_wire(
-            jnp.einsum("th,shd->tsd", hidden, down_full, preferred_element_type=jnp.float32)
-        )
-        .astype(jnp.bfloat16)
-        .reshape(stream.shape[0] * lax.axis_size("tp"), -1),
-        "tp",
-        scatter_dimension=0,
-        tiled=True,
-    ).astype(jnp.float32)
-    return (stream + down_sum).astype(jnp.bfloat16)
+    down_part = jnp.einsum("th,shd->tsd", hidden, down_full, preferred_element_type=jnp.float32)
+    down_part = down_part.astype(jnp.bfloat16).reshape(partial_sum.shape)
+    return tp_call(
+        sum_kernel,
+        2,
+        (down_part, stream),
+        jax.ShapeDtypeStruct(residual.shape, residual.dtype),
+        rows,
+        False,
+    )
 
 
 def solution(mesh):

time: 479 us -> 423 us (0.88)
  waiting for transfers between devices: 84.2 us -> 0 us
  Pallas kernels: 346 us -> 393 us
  between operations: 13.2 us -> 0.12 us
  other arithmetic: 7.12 us -> 1.7 us
    reduce_scatter x2 -> x0, waiting for transfers between devices: 61.7 us -> none  [the longest x1 31.3 us: body(): lax.psum_scatter(to_wire(jnp.einsum('th,shd->tsd', hidden, down_full, pre...]
    pallas_call x0 -> x2, Pallas kernels: none -> 47.2 us  [tp_call(): pl.pallas_call(functools.partial(kernel, tp_count), out_shape=out_shape,...]
    all_gather x1 -> x0, waiting for transfers between devices: 22.5 us -> none  [body(): lax.all_gather(normalize(stream, mixer_gain), 'tp', axis=0, tiled=True)]
  transfers between devices with their start and end apart: 3 -> 0, of which waited for: 3 -> 0; matrix products, arithmetic and copies ran while one was open for 0% -> 0% of each run, Pallas kernels for 0% -> 0%
where the time goes in v2:
time: 423 us; the launch traced here: 422 us
  Pallas kernels  393 us (93%)
  matrix products  18.4 us (4%)
  local copies, waits for them, and re-layouts  9.1 us (2%)
    pallas_call x1, Pallas kernels, mixer(): pl.pallas_call(functools.partial(mixer_kernel, sp_count, ((heads_major, D...  346 us
    pallas_call x2, Pallas kernels, tp_call(): pl.pallas_call(functools.partial(kernel, tp_count), out_shape=out_shape,...  47.2 us
    dot_general x1, matrix products, body(): jnp.einsum('th,shd->tsd', hidden, down_full, preferred_element_type=jnp.f...  16 us

profile of v2, /device:TPU:16, one launch (start us, length us, event | category | flops | bytes accessed | tf_op | source)
XLA Modules:
  0.0 422.4 jit_solution(10502306863031613991)
XLA Ops:
  0.0 0.0 copy-start
  0.0 1.4 copy.18.gain_minor
  1.4 1.4 copy.17.gain_major
  2.8 1.7 pad_maximum_fusion.kv_minor
  4.5 345.9 %shard_map.154 = (bf16[512,256]{1,0:T(8,128)(2,1)}, bf16[512,128]{1,0:T(8,128)(2,1)}, bf16[2048,2048]{1,0:T(8,128)(2,1)}, bf16[8,2048,256]{2,1,0:T(8,128)(2,1)}) custom-call(bf16[512,256]{1,0:T(8,128)(2,1)} %q_major.1, bf16[512,256]{1,0:T(8,128)(2,1)} %k_major.1, bf16[512,256]{1,0:T(8,128)(2,1)} %v_major.1, bf16[512,128]{1,0:T(8,128)(2,1)} %q_minor.1, ...), custom_call_target="tpu_custom_call" | custom-call | tf_op jit(solution)/shard_map/pallas_call | solution.py:283
  350.5 0.0 copy-start.5
  350.5 0.0 copy-start.6
  350.5 0.0 copy-done
  350.5 1.7 fusion.2
  352.2 0.0 copy-done.5
  352.3 0.0 copy-done.6
  352.3 0.0 copy-start.3
  352.3 0.0 copy-start.4
  352.3 0.7 add_convert_fusion.partial
  353.0 0.3 copy-done.3
  353.3 0.0 copy-done.4
  353.3 30.8 %shard_map.155 = (f32[128,2048]{1,0:T(8,128)S(1)}, bf16[512,2048]{1,0:T(8,128)(2,1)S(1)}) custom-call(bf16[512,2048]{1,0:T(8,128)(2,1)S(1)} %add_convert_fusion.partial, bf16[128,2048]{1,0:T(8,128)(2,1)S(1)} %copy-done.3, f32[1,2048]{1,0:T(1,128)S(1)} %bitcast.15), custom_call_target="tpu_custom_call" | custom-call | tf_op jit(solution)/shard_map/pallas_call | solution.py:422
  384.1 0.0 copy-start.1
  384.1 1.0 copy-done.1
  385.1 16.0 %convolution_convert_fusion = bf16[512,8,256]{0,2,1:T(8,128)(2,1)} fusion(bf16[8,2048,256]{2,1,0:T(8,128)(2,1)} %get-tuple-element.15, bf16[512,2048]{1,0:T(8,128)(2,1)S(1)} %get-tuple-element.13, bf16[2048,2048]{1,0:T(8,128)(2,1)} %get-tuple-element.14), kind=kOutput, calls=%fused_computation.3 | convolution fusion | flops 8594128896 | bytes 20971520 | tf_op jit(solution)/shard_map/th,shd->tsd/dot_general | solution.py:488
  401.1 2.9 copy.22.partial
  404.0 0.0 copy-start.2
  404.0 1.2 copy-done.2
  405.2 16.4 %shard_map.156 = bf16[128,2048]{1,0:T(8,128)(2,1)S(1)} custom-call(bf16[512,2048]{1,0:T(8,128)(2,1)S(1)} %copy.22.partial, f32[128,2048]{1,0:T(8,128)S(1)} %copy-done.2), custom_call_target="tpu_custom_call" | custom-call | tf_op jit(solution)/shard_map/pallas_call | solution.py:422
  421.6 0.8 copy.24
Async XLA Ops:
  0.0 350.5 %copy-start = (bf16[256,2048]{1,0:T(8,128)(2,1)S(1)}, bf16[256,2048]{1,0:T(8,128)(2,1)}, u32[]{:S(2)}) copy-start(bf16[256,2048]{1,0:T(8,128)(2,1)} %param.27) | copy-start | bytes 3145732
  350.5 1.8 copy-start.5
  350.5 1.8 copy-start.6
  352.3 1.0 copy-start.3
  352.3 1.0 copy-start.4
  384.1 1.0 copy-start.1
  404.0 1.2 copy-start.2
